TPU v7x, 512 devices: a whole 4x4x16 slice. The times are simulated.
512 devices in a mesh: kv: 16 (over y, x), tp: 32 (over z, core).
Axes of the slice: x: 4, y: 4, z: 16, core: 2. Of those that a mesh axis runs over, the one named last changes fastest.
Arguments:
- residual: bfloat16 [512, 2048], P('tp', 'kv'), may hold values from -64 to 64
- prior_state: float32 [512, 16, 128, 128], P('tp', 'kv'), may hold values from -6 to 6
- w_query: bfloat16 [2048, 2048], P('tp', 'kv'), may hold values from -0.125 to 0.125
- w_forget: bfloat16 [2048, 2048], P('tp', 'kv'), may hold values from -0.125 to 0.125
- w_value: bfloat16 [2048, 2048], P('tp', 'kv'), may hold values from -0.125 to 0.125
- w_outgate: bfloat16 [2048, 2048], P('tp', 'kv'), may hold values from -0.125 to 0.125
- forget_floor: float32 [2048], P('kv'), may hold values from 0.05 to 0.9
- group_gain: float32 [2048], P('kv'), may hold values from 0.1 to 1.9
- w_mix_out: bfloat16 [2048, 2048], P('kv', 'tp'), may hold values from -0.397747564 to 0.397747564
- gain_mix_pre: float32 [2048], replicated, may hold values from 0.1 to 1.9
- gain_mix_post: float32 [2048], replicated, may hold values from 0.05 to 1.9
- gain_mlp_pre: float32 [2048], replicated, may hold values from 0.1 to 1.9
- gain_mlp_post: float32 [2048], replicated, may hold values from 0.1 to 1.9
- w_up: bfloat16 [2048, 8192], P('tp', 'kv'), may hold values from -0.125 to 0.125
- w_down: bfloat16 [8192, 2048], P('kv', 'tp'), may hold values from -0.198873782 to 0.198873782
Outputs:
- layer_out: bfloat16 [512, 2048], P('tp', 'kv')
- new_state: float32 [512, 16, 128, 128], P('tp', 'kv')
All inputs are finite; a program needn't handle non-finite values.
Results may differ from a plain program's by a relative error of at most 0.015.
Values may be sent and summed in bfloat16 or wider, within the bound.
No kernel may reach another device: no remote copies, remote signals or barrier semaphores. Data moves between devices by JAX's collectives and lax.ppermute only.
A program may use at most 64 MiB of HBM per device.

v0:
```python
import jax
import jax.numpy as jnp
from jax import lax
from jax.sharding import Mesh
from jax.sharding import PartitionSpec as P

HEAD_DIM = 128
KV = ("y", "x")
TP = ("z", "c")
epsilon = 1e-06


def inverse_norm(values):
    return lax.rsqrt(jnp.mean(values * values, axis=-1, keepdims=True) + epsilon)


def exchange(blocks, axes):
    return lax.all_to_all(blocks, axes, 0, 0, tiled=True)


def from_everyone(value, axes):
    devices = lax.axis_size(axes)
    return exchange(jnp.broadcast_to(value[None], (devices, *value.shape)), axes)


def shards(
    residual,
    prior_state,
    w_query,
    w_forget,
    w_value,
    w_outgate,
    forget_floor,
    group_gain,
    w_mix_out,
    gain_mix_pre,
    gain_mix_post,
    gain_mlp_pre,
    gain_mlp_post,
    w_up,
    w_down,
):
    batch_rows, own_cols = residual.shape
    groups = lax.axis_size(KV)
    full_width = groups * own_cols
    place = lax.axis_index(KV)
    head_cols = w_query.shape[1]
    hidden = w_up.shape[1]
    own_weights = jnp.concatenate(
        (w_query, w_forget, w_value, w_outgate, w_mix_out.T, w_up, w_down.T), axis=1
    )
    weights = lax.all_gather(own_weights, TP, axis=0, tiled=True)
    at = 4 * head_cols
    w_in = weights[:, :at]
    w_mix = weights[:, at : at + w_mix_out.shape[0]]
    at += w_mix_out.shape[0]
    w_up_all = weights[:, at : at + hidden]
    w_down_all = weights[:, at + hidden :]
    stream = from_everyone(residual, KV).astype(jnp.float32)
    scale = lax.rsqrt(jnp.sum(stream * stream, axis=(0, 2), keepdims=True) / full_width + epsilon)
    normed = (stream * scale * gain_mix_pre.reshape(groups, 1, own_cols)).astype(jnp.bfloat16)
    normed = normed.transpose(1, 0, 2).reshape(batch_rows, full_width)
    pre = jnp.dot(normed, w_in, preferred_element_type=jnp.float32).astype(jnp.bfloat16)
    query_pre, forget_pre, value_pre, gate_pre = (
        p.astype(jnp.float32) for p in jnp.split(pre, 4, axis=1)
    )
    query = jax.nn.silu(query_pre)
    forget = forget_floor + (1.0 - forget_floor) * jax.nn.sigmoid(forget_pre)
    new_state = (
        forget[:, :, None] * prior_state[:, 0] + (1.0 - forget)[:, :, None] * value_pre[:, None, :]
    )
    readout = jnp.einsum("bk,bkv->bv", query, new_state, precision=lax.Precision.HIGHEST)
    gated = (readout * inverse_norm(readout) * group_gain * jax.nn.sigmoid(gate_pre)).astype(
        jnp.bfloat16
    )
    mixed_part = lax.dot_general(
        gated, w_mix, (((1,), (1,)), ((), ())), preferred_element_type=jnp.float32
    )
    mixed = exchange(mixed_part.astype(jnp.bfloat16).reshape(batch_rows, groups, own_cols), KV)
    mixed = jnp.sum(mixed.astype(jnp.float32), axis=0)
    mix_scale = lax.rsqrt(jnp.sum(mixed * mixed) / full_width + epsilon)
    own_row = lax.dynamic_index_in_dim(stream, place, 1, keepdims=False)
    after_row = (own_row + mixed * mix_scale * gain_mix_post.reshape(groups, own_cols)).astype(
        jnp.bfloat16
    )
    after = from_everyone(after_row, KV).astype(jnp.float32)
    after_scale = lax.rsqrt(
        jnp.sum(after * after, axis=(1, 2), keepdims=True) / full_width + epsilon
    )
    hidden_in = (after * after_scale * gain_mlp_pre.reshape(groups, own_cols)).astype(jnp.bfloat16)
    up_sum = jnp.dot(
        hidden_in.reshape(batch_rows, full_width), w_up_all, preferred_element_type=jnp.float32
    )
    squared = jnp.square(jax.nn.relu(up_sum)).astype(jnp.bfloat16)
    channel_part = lax.dot_general(
        squared, w_down_all, (((1,), (1,)), ((), ())), preferred_element_type=jnp.float32
    )
    channel = exchange(
        channel_part.astype(jnp.bfloat16).reshape(batch_rows, groups, own_cols).transpose(1, 0, 2),
        KV,
    )
    channel = jnp.sum(channel.astype(jnp.float32), axis=0)
    out_gain = lax.dynamic_index_in_dim(
        gain_mlp_post.reshape(groups, own_cols), place, 0, keepdims=True
    )
    after_own = lax.dynamic_index_in_dim(after, place, 1, keepdims=False)
    layer_out = (after_own + channel * out_gain).astype(jnp.bfloat16)
    return (layer_out, new_state[:, None])


def solution(mesh):
    grid = Mesh(mesh.devices.reshape(4, 4, 16, 2), (*KV, *TP))
    return jax.shard_map(
        shards,
        mesh=grid,
        in_specs=(
            P(TP, KV),
            P(TP, KV, None, None),
            P(TP, KV),
            P(TP, KV),
            P(TP, KV),
            P(TP, KV),
            P(KV),
            P(KV),
            P(KV, TP),
            P(),
            P(),
            P(),
            P(),
            P(TP, KV),
            P(KV, TP),
        ),
        out_specs=(P(TP, KV), P(TP, KV, None, None)),
        check_vma=False,
    )
```

profile of v0, /device:TPU:32, one launch (start us, length us, event | category | flops | bytes accessed | tf_op | source)
XLA Modules:
  0.0 153.1 jit_solution(12552396937788839422)
XLA Ops:
  7.2 0.0 copy-start
  7.2 0.0 copy-start.2
  7.2 0.0 all-gather.2.cloned.1.call-start
  7.2 0.7 constant_dynamic-update-slice_fusion.5
  8.0 0.7 constant_dynamic-update-slice_fusion.4
  8.7 0.7 constant_dynamic-update-slice_fusion.3
  9.4 0.7 constant_dynamic-update-slice_fusion.2
  10.1 0.7 constant_dynamic-update-slice_fusion.1
  10.9 0.8 constant_dynamic-update-slice_fusion
  11.7 0.8 bitcast_dynamic-update-slice_fusion
  12.6 0.0 copy-start.1
  12.6 0.7 copy-done.1
  13.2 0.0 all-gather.2.cloned.1.call-update
  13.3 1.3 broadcast_in_dim.4
  14.6 7.0 %all-to-all-start = ((bf16[16,16,128]{2,1,0:T(8,128)(2,1)}), bf16[16,16,128]{2,1,0:T(8,128)(2,1)S(1)}, u32[]{:S(2)}, u32[]{:S(2)}) async-start(bf16[16,16,128]{2,1,0:T(8,128)(2,1)} %broadcast_in_dim.4), calls=%async_computation | async-start | bytes 131072 | tf_op jit(solution)/shard_map/all_to_all | solution.py:18
  21.6 0.7 broadcast_subtract_fusion.1
  22.3 0.0 copy-done
  22.3 7.0 %all-to-all-done = bf16[16,16,128]{2,1,0:T(8,128)(2,1)S(1)} async-done(((bf16[16,16,128]{2,1,0:T(8,128)(2,1)}), bf16[16,16,128]{2,1,0:T(8,128)(2,1)S(1)}, u32[]{:S(2)}, u32[]{:S(2)}) %all-to-all-start) | async-done | bytes 65568 | tf_op jit(solution)/shard_map/all_to_all | solution.py:18
  29.3 0.1 multiply_reduce_fusion.1
  29.4 65.2 %all-gather.2.cloned.1.call-done = bf16[2048,1664]{1,0:T(8,128)(2,1)} async-done(((bf16[64,1664]{1,0:T(8,128)(2,1)}), bf16[2048,1664]{1,0:T(8,128)(2,1)}) %all-gather.2.cloned.1.call-update) | async-done | bytes 6815760 | tf_op jit(solution)/shard_map/all_gather | solution.py:52
  94.7 2.0 %fusion.20 = bf16[16,512]{1,0:T(8,128)(2,1)S(1)} fusion(bf16[2048,1664]{1,0:T(8,128)(2,1)} %all-gather.2.cloned.1.call-done, f32[16,128]{1,0:T(8,128)} %bitcast.60, f32[16]{0:T(128)S(1)} %add_rsqrt_fusion.2, bf16[16,16,128]{2,1,0:T(8,128)(2,1)S(1)} %all-to-all-done), kind=kOutput, calls=%fused_computation.12 | convolution fusion | flops 33693696 | bytes 2187328 | tf_op jit(solution)/shard_map/dot_general | solution.py:63
  96.7 0.7 multiply_add_fusion.1
  97.4 2.6 %fusion.24 = f32[16,1,128]{2,1,0:T(1,128)S(1)} fusion(f32[16,128,1]{1,2,0:T(1,128)S(1)} %bitcast.56, f32[16,1,128,128]{3,2,1,0:T(8,128)} %param.16, f32[16,128]{1,0:T(8,128)S(1)} %slice_convert_fusion, f32[16,128]{1,0:T(8,128)S(1)} %get-tuple-element.3, f32[16,128]{1,0:T(8,128)S(1)} %get-tuple-element.2), kind=kOutput, calls=%fused_computation.15 | convolution fusion | flops 3932160 | bytes 1089536 | tf_op jit(solution)/shard_map/bk,bkv->bv/dot_general | solution.py:72
  100.0 0.1 multiply_reduce_fusion.3
  100.1 1.3 fusion.8
  101.5 0.7 copy.24
  102.1 6.8 %all-to-all-start.1 = ((bf16[16,16,128]{2,1,0:T(8,128)(2,1)}), bf16[16,16,128]{2,1,0:T(8,128)(2,1)S(1)}, u32[]{:S(2)}, u32[]{:S(2)}) async-start(bf16[16,16,128]{2,1,0:T(8,128)(2,1)} %bitcast.22), calls=%async_computation.1 | async-start | bytes 131072 | tf_op jit(solution)/shard_map/all_to_all | solution.py:18
  109.0 7.6 %all-to-all-done.1 = bf16[16,16,128]{2,1,0:T(8,128)(2,1)S(1)} async-done(((bf16[16,16,128]{2,1,0:T(8,128)(2,1)}), bf16[16,16,128]{2,1,0:T(8,128)(2,1)S(1)}, u32[]{:S(2)}, u32[]{:S(2)}) %all-to-all-start.1) | async-done | bytes 65568 | tf_op jit(solution)/shard_map/all_to_all | solution.py:18
  116.6 0.6 multiply_reduce_fusion.2
  117.9 0.7 fusion.43
  118.6 0.6 broadcast_in_dim.5
  119.3 3.5 %all-to-all-start.2 = ((bf16[16,16,128]{2,1,0:T(8,128)(2,1)}), bf16[16,16,128]{2,1,0:T(8,128)(2,1)S(1)}, u32[]{:S(2)}, u32[]{:S(2)}) async-start(bf16[16,16,128]{2,1,0:T(8,128)(2,1)} %broadcast_in_dim.5), calls=%async_computation.2 | async-start | bytes 131072 | tf_op jit(solution)/shard_map/all_to_all | solution.py:18
  122.8 2.8 %multiply_add_fusion = f32[16,1,128,128]{3,2,1,0:T(8,128)} fusion(f32[16,1,128,128]{3,2,1,0:T(8,128)} %param.16, f32[16,128]{1,0:T(8,128)S(1)} %slice_convert_fusion, f32[16,128]{1,0:T(8,128)S(1)} %get-tuple-element.3, f32[16,128]{1,0:T(8,128)S(1)} %get-tuple-element.2), kind=kLoop, calls=%fused_computation.16 | loop fusion | flops 786432 | bytes 2121728 | tf_op jit(solution)/shard_map/add | solution.py:70
  125.6 4.8 %all-to-all-done.2 = bf16[16,16,128]{2,1,0:T(8,128)(2,1)S(1)} async-done(((bf16[16,16,128]{2,1,0:T(8,128)(2,1)}), bf16[16,16,128]{2,1,0:T(8,128)(2,1)S(1)}, u32[]{:S(2)}, u32[]{:S(2)}) %all-to-all-start.2) | async-done | bytes 65568 | tf_op jit(solution)/shard_map/all_to_all | solution.py:18
  130.4 0.2 multiply_reduce_fusion
  130.6 0.0 copy-done.2
  130.6 0.1 multiply_convert_fusion
  130.7 3.2 %fusion.5 = bf16[2,16,8,128]{3,2,1,0:T(8,128)(2,1)S(1)} fusion(bf16[2048,1664]{1,0:T(8,128)(2,1)} %all-gather.2.cloned.1.call-done, bf16[2,8,16,128]{3,2,1,0:T(8,128)(2,1)S(1)} %bitcast.53), kind=kOutput, calls=%fused_computation.7 | convolution fusion | flops 67166208 | bytes 4325376 | tf_op jit(solution)/shard_map/dot_general | solution.py:95
  133.9 0.6 copy.36
  134.6 3.5 %all-to-all-start.3 = ((bf16[16,16,128]{2,1,0:T(8,128)(2,1)}), bf16[16,16,128]{2,1,0:T(8,128)(2,1)S(1)}, u32[]{:S(2)}, u32[]{:S(2)}) async-start(bf16[16,16,128]{2,1,0:T(8,128)(2,1)} %bitcast.51), calls=%async_computation.3 | async-start | bytes 131072 | tf_op jit(solution)/shard_map/all_to_all | solution.py:18
  138.1 7.6 %all-to-all-done.3 = bf16[16,16,128]{2,1,0:T(8,128)(2,1)S(1)} async-done(((bf16[16,16,128]{2,1,0:T(8,128)(2,1)}), bf16[16,16,128]{2,1,0:T(8,128)(2,1)S(1)}, u32[]{:S(2)}, u32[]{:S(2)}) %all-to-all-start.3) | async-done | bytes 65568 | tf_op jit(solution)/shard_map/all_to_all | solution.py:18
  145.7 0.6 add_convert_fusion
  (11 shorter events, 0.1 us)
Async XLA Ops:
  7.2 15.1 %copy-start = (f32[2048]{0:T(1024)S(1)}, f32[2048]{0:T(1024)}, u32[]{:S(2)}) copy-start(f32[2048]{0:T(1024)} %param.27) | copy-start | bytes 24580
  7.2 123.4 %copy-start.2 = (f32[2048]{0:T(1024)S(1)}, f32[2048]{0:T(1024)}, u32[]{:S(2)}) copy-start(f32[2048]{0:T(1024)} %param.26) | copy-start | bytes 24580
  7.2 87.5 %all-gather.2.cloned.1.call-start = ((), (), s32[]{:S(2)}) async-start(), calls=%async_computation.4 | async-start | bytes 7028736 | tf_op jit(solution)/shard_map/all_gather | solution.py:52
  12.6 0.7 copy-start.1
  14.6 14.7 %all-to-all-start = ((bf16[16,16,128]{2,1,0:T(8,128)(2,1)}), bf16[16,16,128]{2,1,0:T(8,128)(2,1)S(1)}, u32[]{:S(2)}, u32[]{:S(2)}) async-start(bf16[16,16,128]{2,1,0:T(8,128)(2,1)} %broadcast_in_dim.4), calls=%async_computation | async-start | bytes 131072 | tf_op jit(solution)/shard_map/all_to_all | solution.py:18
  102.1 14.5 %all-to-all-start.1 = ((bf16[16,16,128]{2,1,0:T(8,128)(2,1)}), bf16[16,16,128]{2,1,0:T(8,128)(2,1)S(1)}, u32[]{:S(2)}, u32[]{:S(2)}) async-start(bf16[16,16,128]{2,1,0:T(8,128)(2,1)} %bitcast.22), calls=%async_computation.1 | async-start | bytes 131072 | tf_op jit(solution)/shard_map/all_to_all | solution.py:18
  119.3 11.1 %all-to-all-start.2 = ((bf16[16,16,128]{2,1,0:T(8,128)(2,1)}), bf16[16,16,128]{2,1,0:T(8,128)(2,1)S(1)}, u32[]{:S(2)}, u32[]{:S(2)}) async-start(bf16[16,16,128]{2,1,0:T(8,128)(2,1)} %broadcast_in_dim.5), calls=%async_computation.2 | async-start | bytes 131072 | tf_op jit(solution)/shard_map/all_to_all | solution.py:18
  134.6 11.1 %all-to-all-start.3 = ((bf16[16,16,128]{2,1,0:T(8,128)(2,1)}), bf16[16,16,128]{2,1,0:T(8,128)(2,1)S(1)}, u32[]{:S(2)}, u32[]{:S(2)}) async-start(bf16[16,16,128]{2,1,0:T(8,128)(2,1)} %bitcast.51), calls=%async_computation.3 | async-start | bytes 131072 | tf_op jit(solution)/shard_map/all_to_all | solution.py:18
Sparse Core Ops, SparseCore 0:
  13.4 81.2 all-gather.1
where the time goes:
time: 154 us; the launch traced here: 153 us
  waiting for transfers between devices  92.2 us (60%)
  starting transfers between devices  20.9 us (14%)
  between operations  14.8 us (10%)
  local copies, waits for them, and re-layouts  9.3 us (6%)
  matrix products  9.19 us (6%)
  other arithmetic  6.68 us (4%)
    all_gather x1, waiting for transfers between devices, shards(): weights = lax.all_gather(own_weights, TP, axis=0, tiled=True)  65.2 us
    all_to_all x4, waiting for transfers between devices, exchange(): return lax.all_to_all(blocks, axes, 0, 0, tiled=True)  27 us
    all_to_all x4, starting transfers between devices, exchange(): return lax.all_to_all(blocks, axes, 0, 0, tiled=True)  20.8 us
    unnamed x13, local copies, waits for them, and re-layouts  5.83 us
    dot_general x1, matrix products, shards(): lax.dot_general(squared, w_down_all, (((1,), (1,)), ((), ())), preferred_...  3.21 us
  transfers between devices with their start and end apart: 5, of which 5 were waited for; matrix products, arithmetic and copies ran while one was open for 3% of the time, Pallas kernels for 0%

commit v1 on v0

--- a/solution.py
+++ b/solution.py
@@ -49,7 +49,10 @@
     own_weights = jnp.concatenate(
         (w_query, w_forget, w_value, w_outgate, w_mix_out.T, w_up, w_down.T), axis=1
     )
-    weights = lax.all_gather(own_weights, TP, axis=0, tiled=True)
+    n_dev = lax.axis_size(TP)
+    pieces = jnp.stack([own_weights for _ in range(n_dev)])
+    pieces = lax.all_to_all(pieces, TP, split_axis=0, concat_axis=0)
+    weights = jnp.concatenate(pieces, axis=0)
     at = 4 * head_cols
     w_in = weights[:, :at]
     w_mix = weights[:, at : at + w_mix_out.shape[0]]

time: 154 us -> 386 us (2.51)
  waiting for transfers between devices: 92.2 us -> 325 us
  starting transfers between devices: 20.9 us -> 34.4 us
  between operations: 14.8 us -> 1.54 us
    all_to_all x0 -> x1, waiting for transfers between devices: none -> 302 us  [shards(): pieces = lax.all_to_all(pieces, TP, split_axis=0, concat_axis=0)]
    all_gather x1 -> x0, waiting for transfers between devices: 65.2 us -> none  [shards(): weights = lax.all_gather(own_weights, TP, axis=0, tiled=True)]
    all_to_all x0 -> x1, starting transfers between devices: none -> 15.5 us  [shards(): pieces = lax.all_to_all(pieces, TP, split_axis=0, concat_axis=0)]
  transfers between devices with their start and end apart: 5 -> 5, of which waited for: 5 -> 5; matrix products, arithmetic and copies ran while one was open for 3% -> 2% of each run, Pallas kernels for 0% -> 0%
where the time goes in v1:
time: 386 us; the launch traced here: 385 us
  waiting for transfers between devices  325 us (84%)
  starting transfers between devices  34.4 us (9%)
  local copies, waits for them, and re-layouts  12.4 us (3%)
  matrix products  7.92 us (2%)
    all_to_all x1, waiting for transfers between devices, shards(): pieces = lax.all_to_all(pieces, TP, split_axis=0, concat_axis=0)  302 us
    all_to_all x4, waiting for transfers between devices, exchange(): return lax.all_to_all(blocks, axes, 0, 0, tiled=True)  23.6 us
    all_to_all x4, starting transfers between devices, exchange(): return lax.all_to_all(blocks, axes, 0, 0, tiled=True)  18.9 us
    all_to_all x1, starting transfers between devices, shards(): pieces = lax.all_to_all(pieces, TP, split_axis=0, concat_axis=0)  15.5 us
  transfers between devices with their start and end apart: 5, of which 5 were waited for; matrix products, arithmetic and copies ran while one was open for 2% of the time, Pallas kernels for 0%

profile of v1, /device:TPU:32, one launch (start us, length us, event | category | flops | bytes accessed | tf_op | source)
XLA Modules:
  0.0 384.9 jit_solution(10323041970228822793)
XLA Ops:
  0.6 0.0 copy-start
  0.6 1.3 broadcast_in_dim.4
  2.0 7.0 %all-to-all-start = ((bf16[16,16,128]{2,1,0:T(8,128)(2,1)}), bf16[16,16,128]{2,1,0:T(8,128)(2,1)S(1)}, u32[]{:S(2)}, u32[]{:S(2)}) async-start(bf16[16,16,128]{2,1,0:T(8,128)(2,1)} %broadcast_in_dim.4), calls=%async_computation | async-start | bytes 131072 | tf_op jit(solution)/shard_map/all_to_all | solution.py:18
  9.0 0.7 constant_dynamic-update-slice_fusion.5
  9.7 0.7 constant_dynamic-update-slice_fusion.4
  10.5 0.7 constant_dynamic-update-slice_fusion.3
  11.2 0.7 constant_dynamic-update-slice_fusion.2
  11.9 0.7 constant_dynamic-update-slice_fusion.1
  12.6 0.8 constant_dynamic-update-slice_fusion
  13.5 0.8 bitcast_dynamic-update-slice_fusion
  14.3 2.3 all-to-all-done
  16.7 3.7 stack.2
  20.4 0.0 copy-start.4
  20.4 0.0 copy-start.6
  20.4 0.0 copy-start.1
  20.4 0.0 copy-start.5
  20.4 0.0 copy-start.2
  20.4 15.5 %all-to-all-start.1 = ((bf16[32,64,1664]{2,1,0:T(8,128)(2,1)}), bf16[32,64,1664]{2,1,0:T(8,128)(2,1)}, u32[]{:S(2)}, u32[]{:S(2)}) async-start(bf16[32,64,1664]{2,1,0:T(8,128)(2,1)} %stack.2), calls=%async_computation.1 | async-start | bytes 13631488 | tf_op jit(solution)/shard_map/all_to_all | solution.py:54
  35.9 0.0 copy-start.3
  36.0 0.0 copy-done
  36.0 0.0 copy-done.4
  36.0 0.1 multiply_reduce_fusion.1
  36.2 301.7 %all-to-all-done.1 = bf16[32,64,1664]{2,1,0:T(8,128)(2,1)} async-done(((bf16[32,64,1664]{2,1,0:T(8,128)(2,1)}), bf16[32,64,1664]{2,1,0:T(8,128)(2,1)}, u32[]{:S(2)}, u32[]{:S(2)}) %all-to-all-start.1) | async-done | bytes 6815776 | tf_op jit(solution)/shard_map/all_to_all | solution.py:54
  337.9 0.0 copy-done.6
  337.9 2.0 fusion.20
  339.9 0.0 copy-done.1
  339.9 1.4 fusion.24
  341.3 0.1 multiply_reduce_fusion.3
  341.5 0.0 copy-done.5
  341.5 1.3 fusion.8
  342.8 0.7 copy.24
  343.4 4.9 %all-to-all-start.2 = ((bf16[16,16,128]{2,1,0:T(8,128)(2,1)}), bf16[16,16,128]{2,1,0:T(8,128)(2,1)S(1)}, u32[]{:S(2)}, u32[]{:S(2)}) async-start(bf16[16,16,128]{2,1,0:T(8,128)(2,1)} %bitcast.23), calls=%async_computation.2 | async-start | bytes 131072 | tf_op jit(solution)/shard_map/all_to_all | solution.py:18
  348.3 7.6 %all-to-all-done.2 = bf16[16,16,128]{2,1,0:T(8,128)(2,1)S(1)} async-done(((bf16[16,16,128]{2,1,0:T(8,128)(2,1)}), bf16[16,16,128]{2,1,0:T(8,128)(2,1)S(1)}, u32[]{:S(2)}, u32[]{:S(2)}) %all-to-all-start.2) | async-done | bytes 65568 | tf_op jit(solution)/shard_map/all_to_all | solution.py:18
  356.0 0.6 multiply_reduce_fusion.2
  357.3 0.0 copy-done.2
  357.3 0.6 broadcast_in_dim.5
  358.0 3.5 all-to-all-start.3
  361.5 1.6 multiply_add_fusion
  363.0 6.0 %all-to-all-done.3 = bf16[16,16,128]{2,1,0:T(8,128)(2,1)S(1)} async-done(((bf16[16,16,128]{2,1,0:T(8,128)(2,1)}), bf16[16,16,128]{2,1,0:T(8,128)(2,1)S(1)}, u32[]{:S(2)}, u32[]{:S(2)}) %all-to-all-start.3) | async-done | bytes 65568 | tf_op jit(solution)/shard_map/all_to_all | solution.py:18
  369.1 0.2 multiply_reduce_fusion
  369.3 0.0 copy-done.3
  369.3 0.1 multiply_convert_fusion
  369.4 3.2 fusion.5
  372.6 0.6 copy.36
  373.2 3.5 all-to-all-start.4
  376.8 7.6 %all-to-all-done.4 = bf16[16,16,128]{2,1,0:T(8,128)(2,1)S(1)} async-done(((bf16[16,16,128]{2,1,0:T(8,128)(2,1)}), bf16[16,16,128]{2,1,0:T(8,128)(2,1)S(1)}, u32[]{:S(2)}, u32[]{:S(2)}) %all-to-all-start.4) | async-done | bytes 65568 | tf_op jit(solution)/shard_map/all_to_all | solution.py:18
  384.3 0.6 add_convert_fusion
  (14 shorter events, 0.2 us)
Async XLA Ops:
  0.6 35.3 %copy-start = (f32[2048]{0:T(1024)S(1)}, f32[2048]{0:T(1024)}, u32[]{:S(2)}) copy-start(f32[2048]{0:T(1024)} %param.27) | copy-start | bytes 24580
  2.0 14.7 %all-to-all-start = ((bf16[16,16,128]{2,1,0:T(8,128)(2,1)}), bf16[16,16,128]{2,1,0:T(8,128)(2,1)S(1)}, u32[]{:S(2)}, u32[]{:S(2)}) async-start(bf16[16,16,128]{2,1,0:T(8,128)(2,1)} %broadcast_in_dim.4), calls=%async_computation | async-start | bytes 131072 | tf_op jit(solution)/shard_map/all_to_all | solution.py:18
  20.4 15.6 %copy-start.4 = (f32[128]{0:T(128)S(1)}, f32[128]{0:T(128)}, u32[]{:S(2)}) copy-start(f32[128]{0:T(128)} %param.21) | copy-start | bytes 1540
  20.4 317.5 %copy-start.6 = (f32[2048]{0:T(1024)S(1)}, f32[2048]{0:T(1024)}, u32[]{:S(2)}) copy-start(f32[2048]{0:T(1024)} %param.24) | copy-start | bytes 24580
  20.4 319.5 %copy-start.1 = (f32[16,1,128,128]{3,2,1,0:T(8,128)S(1)}, f32[16,1,128,128]{3,2,1,0:T(8,128)}, u32[]{:S(2)}) copy-start(f32[16,1,128,128]{3,2,1,0:T(8,128)} %param.16) | copy-start | bytes 3145732
  20.4 321.1 %copy-start.5 = (f32[128]{0:T(128)S(1)}, f32[128]{0:T(128)}, u32[]{:S(2)}) copy-start(f32[128]{0:T(128)} %param.22) | copy-start | bytes 1540
  20.4 336.9 %copy-start.2 = (f32[2048]{0:T(1024)S(1)}, f32[2048]{0:T(1024)}, u32[]{:S(2)}) copy-start(f32[2048]{0:T(1024)} %param.25) | copy-start | bytes 24580
  20.4 317.5 %all-to-all-start.1 = ((bf16[32,64,1664]{2,1,0:T(8,128)(2,1)}), bf16[32,64,1664]{2,1,0:T(8,128)(2,1)}, u32[]{:S(2)}, u32[]{:S(2)}) async-start(bf16[32,64,1664]{2,1,0:T(8,128)(2,1)} %stack.2), calls=%async_computation.1 | async-start | bytes 13631488 | tf_op jit(solution)/shard_map/all_to_all | solution.py:54
  35.9 333.3 %copy-start.3 = (f32[2048]{0:T(1024)S(1)}, f32[2048]{0:T(1024)}, u32[]{:S(2)}) copy-start(f32[2048]{0:T(1024)} %param.26) | copy-start | bytes 24580
  343.4 12.5 %all-to-all-start.2 = ((bf16[16,16,128]{2,1,0:T(8,128)(2,1)}), bf16[16,16,128]{2,1,0:T(8,128)(2,1)S(1)}, u32[]{:S(2)}, u32[]{:S(2)}) async-start(bf16[16,16,128]{2,1,0:T(8,128)(2,1)} %bitcast.23), calls=%async_computation.2 | async-start | bytes 131072 | tf_op jit(solution)/shard_map/all_to_all | solution.py:18
  358.0 11.1 %all-to-all-start.3 = ((bf16[16,16,128]{2,1,0:T(8,128)(2,1)}), bf16[16,16,128]{2,1,0:T(8,128)(2,1)S(1)}, u32[]{:S(2)}, u32[]{:S(2)}) async-start(bf16[16,16,128]{2,1,0:T(8,128)(2,1)} %broadcast_in_dim.5), calls=%async_computation.3 | async-start | bytes 131072 | tf_op jit(solution)/shard_map/all_to_all | solution.py:18
  373.2 11.1 %all-to-all-start.4 = ((bf16[16,16,128]{2,1,0:T(8,128)(2,1)}), bf16[16,16,128]{2,1,0:T(8,128)(2,1)S(1)}, u32[]{:S(2)}, u32[]{:S(2)}) async-start(bf16[16,16,128]{2,1,0:T(8,128)(2,1)} %bitcast.52), calls=%async_computation.4 | async-start | bytes 131072 | tf_op jit(solution)/shard_map/all_to_all | solution.py:18
